TPU v7x, 32 devices: a whole 2x2x4 slice. The times are simulated.
32 devices in a mesh: grp: 2 (over y), fs: 4 (over z), tp: 4 (over x, core).
Axes of the slice: x: 2, y: 2, z: 4, core: 2. Of those that a mesh axis runs over, the one named last changes fastest.
Arguments:
- tokens: bfloat16 [2048, 2048], P(('grp', 'fs')), parts along dimension 0, may hold values from -6 to 6
- norm_gain: float32 [2048], P('fs'), may hold values from 0.1 to 1.9
- gate_master: float32 [4, 2048, 1024], P(None, 'fs', 'tp'), may hold values from -0.125 to 0.125
- up_master: float32 [4, 2048, 1024], P(None, 'fs', 'tp'), may hold values from -0.125 to 0.125
- chosen: int32 [2048, 2], P(('grp', 'fs')), parts along dimension 0, may hold values from 0 to 3, all different within a row; in each aligned block of 256 rows (0 to 255, 256 to 511, ...) at most 256 rows name the same one
- affinity: float32 [2048, 2], P(('grp', 'fs')), parts along dimension 0, may hold values from 0.05 to 1
Outputs:
- gate_served: bfloat16 [8, 2048, 1024], P(('grp', 'fs'), None, 'tp'), parts along dimension 0
- up_served: bfloat16 [8, 2048, 1024], P(('grp', 'fs'), None, 'tp'), parts along dimension 0
- hidden: bfloat16 [2048, 2, 1024], P(('grp', 'fs'), None, 'tp'), parts along dimension 0
There are 2 independent parts, one for each index of `grp`. A program takes and returns all parts, laid end to end along the dimension named above; an argument that names none is the same for every part. Nothing has to cross between parts.
Inputs may be any that keep to these rules, and one draw needn't show every extreme that they name: Among the rows of one index of fs (256 tokens, all their choices) no expert is chosen more than 256 times, a bound that some block reaches; the choices of one token differ.
All inputs are finite; a program needn't handle non-finite values.
Results may differ from a plain program's by a relative error of at most 0.023.
Values may be sent and summed in bfloat16 or wider, within the bound.
A program may use at most 64 MiB of HBM per device.

v0:
```python
import jax
import jax.numpy as jnp
from jax import lax
from jax.sharding import PartitionSpec as P


def on_device(tokens, norm_gain, gate_master, up_master, chosen, affinity):
    folded_gate = (gate_master * norm_gain[None, :, None]).astype(jnp.bfloat16)
    folded_up = (up_master * norm_gain[None, :, None]).astype(jnp.bfloat16)
    new_gate, new_up = (
        lax.all_to_all(folded_gate, "fs", split_axis=0, concat_axis=1, tiled=True),
        lax.all_to_all(folded_up, "fs", split_axis=0, concat_axis=1, tiled=True),
    )
    experts_all = gate_master.shape[0]
    tok_rows, width = tokens.shape
    top = chosen.shape[1]
    capacity = tok_rows * top * 2 // experts_all
    local = new_gate.shape[0]
    xfloat = tokens.astype(jnp.float32)
    scale = lax.rsqrt(jnp.mean(xfloat * xfloat, axis=-1) + 1e-06)
    share = affinity / jnp.sum(affinity, axis=-1, keepdims=True)
    flat_e = chosen.reshape(-1)
    onehot = (flat_e[:, None] == jnp.arange(experts_all, dtype=jnp.int32)[None, :]).astype(
        jnp.int32
    )
    slot = jnp.sum((jnp.cumsum(onehot, axis=0) - onehot) * onehot, axis=1)
    target = flat_e * capacity + slot
    owner = jnp.repeat(jnp.arange(tok_rows, dtype=jnp.int32), top)
    total = experts_all * capacity
    scale_buf = (
        jnp.zeros((total,), jnp.float32).at[target].set(scale[owner]).reshape(experts_all, capacity)
    )
    share_buf = (
        jnp.zeros((total,), jnp.float32)
        .at[target]
        .set(share.reshape(-1))
        .reshape(experts_all, capacity)
    )
    narrow = width // lax.axis_size("tp")
    own_cols = lax.dynamic_slice_in_dim(tokens, lax.axis_index("tp") * narrow, narrow, 1)
    row_buf = jnp.zeros((total, narrow), jnp.bfloat16).at[target].set(own_cols[owner])
    row_buf = row_buf.reshape(experts_all, capacity, narrow)
    got_rows, got_scale, got_share = (
        lax.all_to_all(row_buf, "fs", split_axis=0, concat_axis=0, tiled=True),
        lax.all_to_all(
            scale_buf.astype(jnp.bfloat16), "fs", split_axis=0, concat_axis=0, tiled=True
        ).astype(scale_buf.dtype),
        lax.all_to_all(
            share_buf.astype(jnp.bfloat16), "fs", split_axis=0, concat_axis=0, tiled=True
        ).astype(share_buf.dtype),
    )
    sources = got_rows.shape[0] // local
    got_rows = got_rows.reshape(sources, local, capacity, narrow)
    piece = lax.all_gather(got_rows, "tp", axis=3, tiled=True)
    more_gate = jnp.einsum("secd,edf->secf", piece, new_gate, preferred_element_type=jnp.float32)
    more_up = jnp.einsum("secd,edf->secf", piece, new_up, preferred_element_type=jnp.float32)
    gate = more_gate
    up = more_up
    factor = got_scale.reshape(sources, local, capacity)[..., None]
    weight = got_share.reshape(sources, local, capacity)[..., None]
    gate = gate * factor
    up = up * factor
    hidden_rows = (weight * jax.nn.silu(gate) * up).astype(jnp.bfloat16)
    hidden_rows = hidden_rows.reshape(sources * local, capacity, hidden_rows.shape[3])
    back = lax.all_to_all(hidden_rows, "fs", split_axis=0, concat_axis=0, tiled=True)
    picked = back.reshape(total, back.shape[2])[target].reshape(tok_rows, top, back.shape[2])
    return (new_gate, new_up, picked)


def solution(mesh):
    return jax.shard_map(
        on_device,
        mesh=mesh,
        in_specs=(
            P(("grp", "fs"), None),
            P("fs"),
            P(None, "fs", "tp"),
            P(None, "fs", "tp"),
            P(("grp", "fs"), None),
            P(("grp", "fs"), None),
        ),
        out_specs=(
            P(("grp", "fs"), None, "tp"),
            P(("grp", "fs"), None, "tp"),
            P(("grp", "fs"), None, "tp"),
        ),
        check_vma=False,
    )
```

profile of v0, /device:TPU:0, one launch (start us, length us, event | category | flops | bytes accessed | tf_op | source)
XLA Modules:
  0.0 163.8 jit_solution(18356809726918053598)
XLA Ops:
  7.2 0.7 broadcast_multiply_fusion
  7.9 0.8 copy.26
  9.3 1.2 reduce-window.6
  10.5 0.2 slice_reduce_fusion
  11.2 1.0 constant_dynamic-slice_fusion
  12.2 5.0 %scatter_custom_fusion.1 = bf16[1024,512]{1,0:T(8,128)(2,1)S(1)} fusion(s32[512]{0:T(512)S(1)} %bitcast.83, bf16[256,512]{1,0:T(8,128)(2,1)S(1)} %constant_dynamic-slice_fusion, s32[1024]{0:T(1024)S(1)} %pad_clamp_fusion.1, bf16[]{:T(256)} %constant.15.clone.1), kind=kCustom, calls=%fused_computation.18 | custom fusion | bytes 1048578 | tf_op jit(solution)/shard_map/scatter | solution.py:41
  17.3 32.0 %all_to_all.46 = bf16[4,256,512]{2,1,0:T(8,128)(2,1)} all-to-all(bf16[4,256,512]{2,1,0:T(8,128)(2,1)S(1)} %bitcast.82), channel_id=1, replica_groups=mesh['grp'=2,'fs'=4,'tp'=4] {'fs'}, dimensions={0} | all-to-all | bytes 2097152 | tf_op jit(solution)/shard_map/all_to_all | solution.py:44
  49.6 2.4 %scatter_custom_fusion = f32[1024]{0:T(1024)S(1)} fusion(s32[512]{0:T(512)S(1)} %bitcast.84, f32[512]{0:T(512)S(1)} %reshape.212, f32[]{:T(128)} %constant.11.clone.1), kind=kCustom, calls=%fused_computation.38 | custom fusion | bytes 4100 | tf_op jit(solution)/shard_map/scatter | solution.py:36
  52.1 0.5 broadcast.103
  52.6 0.7 reduce.3
  53.3 0.6 reshape.249
  53.9 3.2 %all-to-all-start.2 = ((bf16[4,2,128]{2,1,0:T(2,128)(2,1)}), bf16[4,2,128]{2,1,0:T(2,128)(2,1)S(1)}, u32[]{:S(2)}, u32[]{:S(2)}) async-start(bf16[4,2,128]{2,1,0:T(2,128)(2,1)} %reshape.249), calls=%async_computation.2 | async-start | bytes 4096 | tf_op jit(solution)/shard_map/all_to_all | solution.py:48
  57.1 0.3 multiply_reduce_fusion
  57.4 3.5 %gather_fusion = f32[512]{0:T(512)S(1)} fusion(f32[256]{0:T(256)S(1)} %add_rsqrt_fusion, s32[1024]{0:T(1024)S(1)} %pad_clamp_fusion.1), kind=kCustom, calls=%fused_computation.1 | custom fusion | bytes 6144 | tf_op jit(solution)/shard_map/gather | solution.py:31
  61.0 2.4 %scatter_custom_fusion.2 = f32[1024]{0:T(1024)S(1)} fusion(s32[512]{0:T(512)S(1)} %bitcast.85, f32[512]{0:T(512)S(1)} %gather_fusion, f32[]{:T(128)} %constant.11.clone.1), kind=kCustom, calls=%fused_computation.36 | custom fusion | bytes 4100 | tf_op jit(solution)/shard_map/scatter | solution.py:31
  63.4 0.7 reduce.2
  64.1 0.6 reshape.247
  64.7 5.0 %all-to-all-start.4 = ((bf16[4,2,128]{2,1,0:T(2,128)(2,1)}), bf16[4,2,128]{2,1,0:T(2,128)(2,1)S(1)}, u32[]{:S(2)}, u32[]{:S(2)}) async-start(bf16[4,2,128]{2,1,0:T(2,128)(2,1)} %reshape.247), calls=%async_computation.4 | async-start | bytes 4096 | tf_op jit(solution)/shard_map/all_to_all | solution.py:45
  69.7 3.5 %multiply_convert_fusion = (bf16[4,512,256]{2,1,0:T(8,128)(2,1)}, bf16[4,512,256]{2,1,0:T(8,128)(2,1)S(1)}) fusion(f32[4,512,256]{2,1,0:T(8,128)} %param.9, f32[512]{0:T(512)S(1)} %copy-done.2, f32[4,512,256]{2,1,0:T(8,128)} %param.8), kind=kLoop, calls=%fused_computation.7 | loop fusion | flops 2097152 | bytes 6293504 | tf_op jit(solution)/shard_map/convert_element_type | solution.py:9
  73.3 2.0 %all-to-all-done.4 = bf16[4,2,128]{2,1,0:T(2,128)(2,1)S(1)} async-done(((bf16[4,2,128]{2,1,0:T(2,128)(2,1)}), bf16[4,2,128]{2,1,0:T(2,128)(2,1)S(1)}, u32[]{:S(2)}, u32[]{:S(2)}) %all-to-all-start.4) | async-done | bytes 2080 | tf_op jit(solution)/shard_map/all_to_all | solution.py:45
  75.2 26.7 %all_to_all.47 = bf16[4,512,256]{2,1,0:T(8,128)(2,1)S(1)} all-to-all(bf16[4,512,256]{2,1,0:T(8,128)(2,1)S(1)} %get-tuple-element.4), channel_id=1, replica_groups=mesh['grp'=2,'fs'=4,'tp'=4] {'fs'}, dimensions={0} | all-to-all | bytes 2097152 | tf_op jit(solution)/shard_map/all_to_all | solution.py:11
  101.9 3.7 %all-to-all-start.1 = ((bf16[4,512,256]{2,1,0:T(8,128)(2,1)}), bf16[4,512,256]{2,1,0:T(8,128)(2,1)S(1)}, u32[]{:S(2)}, u32[]{:S(2)}) async-start(bf16[4,512,256]{2,1,0:T(8,128)(2,1)} %get-tuple-element.3), calls=%async_computation.1 | async-start | bytes 2097152 | tf_op jit(solution)/shard_map/all_to_all | solution.py:12
  105.7 3.5 %fusion.3 = f32[4,1,256,256]{2,3,0,1:T(8,128)S(1)} fusion(bf16[2048,256,1]{1,0,2:T(8,128)(2,1)S(1)} %bitcast.78, bf16[4,256,2048]{2,1,0:T(8,128)(2,1)} %all-gather.3.cloned.1.call-done, f32[4,256]{1,0:T(4,128)S(1)} %bitcast.91), kind=kOutput, calls=%fused_computation.14 | convolution fusion | flops 1074003968 | bytes 6295552 | tf_op jit(solution)/shard_map/secd,edf->secf/dot_general | solution.py:55
  109.2 20.8 %all-to-all-done.1 = bf16[4,512,256]{2,1,0:T(8,128)(2,1)S(1)} async-done(((bf16[4,512,256]{2,1,0:T(8,128)(2,1)}), bf16[4,512,256]{2,1,0:T(8,128)(2,1)S(1)}, u32[]{:S(2)}, u32[]{:S(2)}) %all-to-all-start.1) | async-done | bytes 1048608 | tf_op jit(solution)/shard_map/all_to_all | solution.py:12
  130.1 4.5 %fusion.6 = bf16[4,256,256]{1,2,0:T(8,128)(2,1)} fusion(bf16[2048,256,1]{1,0,2:T(8,128)(2,1)S(1)} %bitcast.80, bf16[4,256,2048]{2,1,0:T(8,128)(2,1)} %all-gather.3.cloned.1.call-done, f32[4,1,256,256]{2,3,0,1:T(8,128)S(1)} %fusion.3, f32[4,256]{1,0:T(4,128)S(1)} %bitcast.92, f32[4,256]{1,0:T(4,128)S(1)} %bitcast.90), kind=kOutput, calls=%fused_computation.17 | convolution fusion | flops 1075838976 | bytes 6823936 | tf_op jit(solution)/shard_map/secd,edf->secf/dot_general | solution.py:56
  134.6 3.5 %all-to-all-start.5 = ((bf16[4,256,256]{1,2,0:T(8,128)(2,1)}), bf16[4,256,256]{1,2,0:T(8,128)(2,1)S(1)}, u32[]{:S(2)}, u32[]{:S(2)}) async-start(bf16[4,256,256]{1,2,0:T(8,128)(2,1)} %fusion.6), calls=%async_computation.5 | async-start | bytes 1048576 | tf_op jit(solution)/shard_map/all_to_all | solution.py:65
  138.1 14.0 %all-to-all-done.5 = bf16[4,256,256]{1,2,0:T(8,128)(2,1)S(1)} async-done(((bf16[4,256,256]{1,2,0:T(8,128)(2,1)}), bf16[4,256,256]{1,2,0:T(8,128)(2,1)S(1)}, u32[]{:S(2)}, u32[]{:S(2)}) %all-to-all-start.5) | async-done | bytes 524320 | tf_op jit(solution)/shard_map/all_to_all | solution.py:65
  152.1 0.2 copy.33
  152.3 2.0 %gather_fusion.1 = bf16[512,256]{1,0:T(8,128)(2,1)S(1)} fusion(bf16[1024,256]{1,0:T(8,128)(2,1)S(1)} %bitcast.77, s32[1024]{0:T(1024)S(1)} %pad_clamp_fusion), kind=kCustom, calls=%fused_computation.2 | custom fusion | bytes 526336 | tf_op jit(solution)/shard_map/gather | solution.py:66
  154.2 0.8 reshape.181
  155.0 1.0 copy.46
  156.0 1.0 copy.47
  (37 shorter events, 1.5 us)
Async XLA Ops:
  7.2 98.6 %all-gather.3.cloned.1.call-start = ((), (), s32[]{:S(2)}) async-start(), calls=%async_computation.6 | async-start | bytes 5242880 | tf_op jit(solution)/shard_map/all_gather | solution.py:54
  12.2 37.1 %copy-start.1 = (f32[256,2]{0,1:T(2,128)S(1)}, f32[256,2]{0,1:T(2,128)}, u32[]{:S(2)}) copy-start(f32[256,2]{0,1:T(2,128)} %param.11) | copy-start | bytes 6148
  12.2 44.9 %copy-start = (bf16[256,2048]{1,0:T(8,128)(2,1)S(1)}, bf16[256,2048]{1,0:T(8,128)(2,1)}, u32[]{:S(2)}) copy-start(bf16[256,2048]{1,0:T(8,128)(2,1)} %param.6) | copy-start | bytes 3145732
  49.3 20.5 %copy-start.2 = (f32[512]{0:T(512)S(1)}, f32[512]{0:T(512)}, u32[]{:S(2)}) copy-start(f32[512]{0:T(512)} %param.7) | copy-start | bytes 6148
  53.9 10.8 %all-to-all-start.2 = ((bf16[4,2,128]{2,1,0:T(2,128)(2,1)}), bf16[4,2,128]{2,1,0:T(2,128)(2,1)S(1)}, u32[]{:S(2)}, u32[]{:S(2)}) async-start(bf16[4,2,128]{2,1,0:T(2,128)(2,1)} %reshape.249), calls=%async_computation.2 | async-start | bytes 4096 | tf_op jit(solution)/shard_map/all_to_all | solution.py:48
  64.7 10.5 %all-to-all-start.4 = ((bf16[4,2,128]{2,1,0:T(2,128)(2,1)}), bf16[4,2,128]{2,1,0:T(2,128)(2,1)S(1)}, u32[]{:S(2)}, u32[]{:S(2)}) async-start(bf16[4,2,128]{2,1,0:T(2,128)(2,1)} %reshape.247), calls=%async_computation.4 | async-start | bytes 4096 | tf_op jit(solution)/shard_map/all_to_all | solution.py:45
  101.9 28.1 %all-to-all-start.1 = ((bf16[4,512,256]{2,1,0:T(8,128)(2,1)}), bf16[4,512,256]{2,1,0:T(8,128)(2,1)S(1)}, u32[]{:S(2)}, u32[]{:S(2)}) async-start(bf16[4,512,256]{2,1,0:T(8,128)(2,1)} %get-tuple-element.3), calls=%async_computation.1 | async-start | bytes 2097152 | tf_op jit(solution)/shard_map/all_to_all | solution.py:12
  134.6 17.5 %all-to-all-start.5 = ((bf16[4,256,256]{1,2,0:T(8,128)(2,1)}), bf16[4,256,256]{1,2,0:T(8,128)(2,1)S(1)}, u32[]{:S(2)}, u32[]{:S(2)}) async-start(bf16[4,256,256]{1,2,0:T(8,128)(2,1)} %fusion.6), calls=%async_computation.5 | async-start | bytes 1048576 | tf_op jit(solution)/shard_map/all_to_all | solution.py:65
Sparse Core Ops, SparseCore 0:
  49.4 33.5 all-gather.2
where the time goes:
time: 164 us
  blocking collectives  58.7 us (36%)
  waiting for transfers between devices  36.8 us (22%)
  local copies, waits for them, and re-layouts  23.1 us (14%)
  starting transfers between devices  15.5 us (9%)
  between operations  14.3 us (9%)
  matrix products  7.99 us (5%)
  other arithmetic  7.42 us (5%)
    all_to_all x1, blocking collectives, on_device(): lax.all_to_all(row_buf, 'fs', split_axis=0, concat_axis=0, tiled=True)  32 us
    all_to_all x1, blocking collectives, on_device(): lax.all_to_all(folded_gate, 'fs', split_axis=0, concat_axis=1, tiled=True)  26.7 us
    all_to_all x1, waiting for transfers between devices, on_device(): lax.all_to_all(folded_up, 'fs', split_axis=0, concat_axis=1, tiled=True)  20.8 us
    all_to_all x1, waiting for transfers between devices, on_device(): lax.all_to_all(hidden_rows, 'fs', split_axis=0, concat_axis=0, tiled=True)  14 us
    all_to_all x1, starting transfers between devices, on_device(): lax.all_to_all(scale_buf.astype(jnp.bfloat16), 'fs', split_axis=0, concat...  5.05 us
    scatter x1, local copies, waits for them, and re-layouts, on_device(): jnp.zeros((total, narrow), jnp.bfloat16).at[target].set(own_cols[owner])  5.05 us
    dot_general x1, matrix products, on_device(): jnp.einsum('secd,edf->secf', piece, new_up, preferred_element_type=jnp.fl...  4.48 us
    unnamed x15, local copies, waits for them, and re-layouts  3.97 us
  transfers between devices with their start and end apart: 5, of which 3 were waited for; matrix products, arithmetic and copies ran while one was open for 12% of the time, Pallas kernels for 0%

commit v1 on v0

--- a/solution.py
+++ b/solution.py
@@ -2,6 +2,24 @@
 import jax.numpy as jnp
 from jax import lax
 from jax.sharding import PartitionSpec as P
+
+
+def list_vectors(which_axis, axis_k, axis_no, my_data):
+    d_next, value_now = (lax.axis_size(which_axis), lax.axis_index(which_axis))
+    heard = list(my_data.shape)
+    odd = my_data.shape[axis_k] // d_next
+    heard[axis_k] = odd
+    item_now = heard[axis_no]
+    heard[axis_no] = item_now * d_next
+    s_next = jnp.zeros(heard, my_data.dtype)
+    for b in [*range(d_next)]:
+        carry_out = lax.dynamic_slice_in_dim(my_data, (value_now ^ b) * odd, odd, axis=axis_k)
+        if b:
+            carry_out = lax.ppermute(carry_out, which_axis, [(i0, i0 ^ b) for i0 in range(d_next)])
+        s_next = lax.dynamic_update_slice_in_dim(
+            s_next, carry_out, (value_now ^ b) * item_now, axis=axis_no
+        )
+    return s_next
 
 
 def on_device(tokens, norm_gain, gate_master, up_master, chosen, affinity):
@@ -62,7 +80,7 @@
     up = up * factor
     hidden_rows = (weight * jax.nn.silu(gate) * up).astype(jnp.bfloat16)
     hidden_rows = hidden_rows.reshape(sources * local, capacity, hidden_rows.shape[3])
-    back = lax.all_to_all(hidden_rows, "fs", split_axis=0, concat_axis=0, tiled=True)
+    back = list_vectors("fs", 0, 0, hidden_rows)
     picked = back.reshape(total, back.shape[2])[target].reshape(tok_rows, top, back.shape[2])
     return (new_gate, new_up, picked)
 

time: 164 us -> 159 us (0.970)
  waiting for transfers between devices: 36.8 us -> 31.4 us
    all_to_all x1 -> x0, waiting for transfers between devices: 14 us -> none  [on_device(): lax.all_to_all(hidden_rows, 'fs', split_axis=0, concat_axis=0, tiled=True)]
    ppermute x0 -> x3, waiting for transfers between devices: none -> 8.08 us  [list_vectors(): lax.ppermute(carry_out, which_axis, [(i0, i0 ^ b) for i0 in range(d_next)])]
    ppermute x0 -> x3, starting transfers between devices: none -> 4.38 us  [list_vectors(): lax.ppermute(carry_out, which_axis, [(i0, i0 ^ b) for i0 in range(d_next)])]
    all_to_all x1 -> x0, starting transfers between devices: 3.47 us -> none  [on_device(): lax.all_to_all(hidden_rows, 'fs', split_axis=0, concat_axis=0, tiled=True)]
    all_to_all x1, waiting for transfers between devices: 0.01 us -> 1.95 us  [on_device(): lax.all_to_all(share_buf.astype(jnp.bfloat16), 'fs', split_axis=0, concat...]
    all_to_all x1, starting transfers between devices: 5.05 us -> 3.22 us  [on_device(): lax.all_to_all(scale_buf.astype(jnp.bfloat16), 'fs', split_axis=0, concat...]
  transfers between devices with their start and end apart: 5 -> 7, of which waited for: 3 -> 5; matrix products, arithmetic and copies ran while one was open for 12% -> 13% of each run, Pallas kernels for 0% -> 0%
where the time goes in v1:
time: 159 us
  blocking collectives  58.7 us (37%)
  waiting for transfers between devices  31.4 us (20%)
  local copies, waits for them, and re-layouts  23.7 us (15%)
  starting transfers between devices  15 us (9%)
  between operations  14.3 us (9%)
  matrix products  8.21 us (5%)
  other arithmetic  7.41 us (5%)
    all_to_all x1, blocking collectives, on_device(): lax.all_to_all(row_buf, 'fs', split_axis=0, concat_axis=0, tiled=True)  32 us
    all_to_all x1, blocking collectives, on_device(): lax.all_to_all(folded_gate, 'fs', split_axis=0, concat_axis=1, tiled=True)  26.7 us
    all_to_all x1, waiting for transfers between devices, on_device(): lax.all_to_all(folded_up, 'fs', split_axis=0, concat_axis=1, tiled=True)  19.9 us
    ppermute x3, waiting for transfers between devices, list_vectors(): lax.ppermute(carry_out, which_axis, [(i0, i0 ^ b) for i0 in range(d_next)])  8.08 us
    scatter x1, local copies, waits for them, and re-layouts, on_device(): jnp.zeros((total, narrow), jnp.bfloat16).at[target].set(own_cols[owner])  5.05 us
    dot_general x1, matrix products, on_device(): jnp.einsum('secd,edf->secf', piece, new_gate, preferred_element_type=jnp....  4.41 us
    ppermute x3, starting transfers between devices, list_vectors(): lax.ppermute(carry_out, which_axis, [(i0, i0 ^ b) for i0 in range(d_next)])  4.38 us
    unnamed x15, local copies, waits for them, and re-layouts  3.97 us
  transfers between devices with their start and end apart: 7, of which 5 were waited for; matrix products, arithmetic and copies ran while one was open for 13% of the time, Pallas kernels for 0%

profile of v1, /device:TPU:0, one launch (start us, length us, event | category | flops | bytes accessed | tf_op | source)
XLA Modules:
  0.0 158.7 jit_solution(7901068330641729198)
XLA Ops:
  7.2 0.8 copy.18
  8.3 0.7 broadcast_multiply_fusion
  9.0 1.2 reduce-window.6
  11.2 1.0 constant_dynamic-slice_fusion
  12.2 5.0 %scatter_custom_fusion.1 = bf16[1024,512]{1,0:T(8,128)(2,1)S(1)} fusion(s32[512]{0:T(512)S(1)} %bitcast.80, bf16[256,512]{1,0:T(8,128)(2,1)S(1)} %constant_dynamic-slice_fusion, s32[1024]{0:T(1024)S(1)} %pad_clamp_fusion.1, bf16[]{:T(256)} %constant.16.clone.1), kind=kCustom, calls=%fused_computation.17 | custom fusion | bytes 1048578 | tf_op jit(solution)/shard_map/scatter | solution.py:59
  17.2 32.0 %all_to_all.41 = bf16[4,256,512]{2,1,0:T(8,128)(2,1)} all-to-all(bf16[4,256,512]{2,1,0:T(8,128)(2,1)S(1)} %bitcast.79), channel_id=1, replica_groups=mesh['grp'=2,'fs'=4,'tp'=4] {'fs'}, dimensions={0} | all-to-all | bytes 2097152 | tf_op jit(solution)/shard_map/all_to_all | solution.py:62
  49.6 3.5 %gather_fusion = f32[512]{0:T(512)S(1)} fusion(f32[256]{0:T(256)S(1)} %add_rsqrt_fusion, s32[1024]{0:T(1024)S(1)} %pad_clamp_fusion.1), kind=kCustom, calls=%fused_computation.1 | custom fusion | bytes 6144 | tf_op jit(solution)/shard_map/gather | solution.py:49
  53.1 2.4 %scatter_custom_fusion.2 = f32[1024]{0:T(1024)S(1)} fusion(s32[512]{0:T(512)S(1)} %bitcast.81, f32[512]{0:T(512)S(1)} %gather_fusion, f32[]{:T(128)} %constant.17.clone.1), kind=kCustom, calls=%fused_computation.43 | custom fusion | bytes 4100 | tf_op jit(solution)/shard_map/scatter | solution.py:49
  56.1 0.7 reduce.2
  56.8 0.6 reshape.248
  57.3 3.2 %all-to-all-start.4 = ((bf16[4,2,128]{2,1,0:T(2,128)(2,1)}), bf16[4,2,128]{2,1,0:T(2,128)(2,1)S(1)}, u32[]{:S(2)}, u32[]{:S(2)}) async-start(bf16[4,2,128]{2,1,0:T(2,128)(2,1)} %reshape.248), calls=%async_computation.4 | async-start | bytes 4096 | tf_op jit(solution)/shard_map/all_to_all | solution.py:63
  60.9 2.4 %scatter_custom_fusion = f32[1024]{0:T(1024)S(1)} fusion(s32[512]{0:T(512)S(1)} %bitcast.82, f32[512]{0:T(512)S(1)} %reshape.213, f32[]{:T(128)} %constant.17.clone.1), kind=kCustom, calls=%fused_computation.45 | custom fusion | bytes 4100 | tf_op jit(solution)/shard_map/scatter | solution.py:54
  63.4 0.7 reduce.3
  64.1 0.6 reshape.250
  64.6 1.4 all-to-all-done.4
  66.0 3.7 %all-to-all-start.2 = ((bf16[4,2,128]{2,1,0:T(2,128)(2,1)}), bf16[4,2,128]{2,1,0:T(2,128)(2,1)S(1)}, u32[]{:S(2)}, u32[]{:S(2)}) async-start(bf16[4,2,128]{2,1,0:T(2,128)(2,1)} %reshape.250), calls=%async_computation.2 | async-start | bytes 4096 | tf_op jit(solution)/shard_map/all_to_all | solution.py:66
  69.7 3.5 %multiply_convert_fusion = (bf16[4,512,256]{2,1,0:T(8,128)(2,1)}, bf16[4,512,256]{2,1,0:T(8,128)(2,1)S(1)}) fusion(f32[4,512,256]{2,1,0:T(8,128)} %param.9, f32[512]{0:T(512)S(1)} %copy-done.2, f32[4,512,256]{2,1,0:T(8,128)} %param.8), kind=kLoop, calls=%fused_computation.7 | loop fusion | flops 2097152 | bytes 6293504 | tf_op jit(solution)/shard_map/convert_element_type | solution.py:27
  73.2 2.0 %all-to-all-done.2 = bf16[4,2,128]{2,1,0:T(2,128)(2,1)S(1)} async-done(((bf16[4,2,128]{2,1,0:T(2,128)(2,1)}), bf16[4,2,128]{2,1,0:T(2,128)(2,1)S(1)}, u32[]{:S(2)}, u32[]{:S(2)}) %all-to-all-start.2) | async-done | bytes 2080 | tf_op jit(solution)/shard_map/all_to_all | solution.py:66
  75.2 26.7 %all_to_all.42 = bf16[4,512,256]{2,1,0:T(8,128)(2,1)S(1)} all-to-all(bf16[4,512,256]{2,1,0:T(8,128)(2,1)S(1)} %get-tuple-element.7), channel_id=1, replica_groups=mesh['grp'=2,'fs'=4,'tp'=4] {'fs'}, dimensions={0} | all-to-all | bytes 2097152 | tf_op jit(solution)/shard_map/all_to_all | solution.py:29
  101.9 3.7 %all-to-all-start.1 = ((bf16[4,512,256]{2,1,0:T(8,128)(2,1)}), bf16[4,512,256]{2,1,0:T(8,128)(2,1)S(1)}, u32[]{:S(2)}, u32[]{:S(2)}) async-start(bf16[4,512,256]{2,1,0:T(8,128)(2,1)} %get-tuple-element.6), calls=%async_computation.1 | async-start | bytes 2097152 | tf_op jit(solution)/shard_map/all_to_all | solution.py:30
  105.7 4.4 %fusion.3 = f32[4,1,256,256]{3,2,0,1:T(8,128)} fusion(bf16[2048,256,1]{1,0,2:T(8,128)(2,1)S(1)} %bitcast.75, bf16[4,256,2048]{2,1,0:T(8,128)(2,1)} %all-gather.3.cloned.1.call-done, f32[4,256]{1,0:T(4,128)S(1)} %bitcast.87), kind=kOutput, calls=%fused_computation.14 | convolution fusion | flops 1074003968 | bytes 6295552 | tf_op jit(solution)/shard_map/secd,edf->secf/dot_general | solution.py:73
  110.1 19.9 %all-to-all-done.1 = bf16[4,512,256]{2,1,0:T(8,128)(2,1)S(1)} async-done(((bf16[4,512,256]{2,1,0:T(8,128)(2,1)}), bf16[4,512,256]{2,1,0:T(8,128)(2,1)S(1)}, u32[]{:S(2)}, u32[]{:S(2)}) %all-to-all-start.1) | async-done | bytes 1048608 | tf_op jit(solution)/shard_map/all_to_all | solution.py:30
  130.1 3.8 %fusion.5 = bf16[4,1,256,256]{3,2,0,1:T(8,128)(2,1)S(1)} fusion(bf16[2048,256,1]{1,0,2:T(8,128)(2,1)S(1)} %bitcast.77, bf16[4,256,2048]{2,1,0:T(8,128)(2,1)} %all-gather.3.cloned.1.call-done, f32[4,1,256,256]{3,2,0,1:T(8,128)} %fusion.3, f32[4,256]{1,0:T(4,128)S(1)} %bitcast.88, f32[4,256]{1,0:T(4,128)S(1)} %bitcast.89), kind=kOutput, calls=%fused_computation.16 | convolution fusion | flops 1075838976 | bytes 6823936 | tf_op jit(solution)/shard_map/secd,edf->secf/dot_general | solution.py:74
  133.9 0.7 dynamic-slice_bitcast_fusion
  134.6 2.0 %collective-permute-start.1 = (bf16[1,256,256]{2,1,0:T(8,128)(2,1)S(1)}, bf16[1,256,256]{2,1,0:T(8,128)(2,1)S(1)}, u32[]{:S(2)}, u32[]{:S(2)}) collective-permute-start(bf16[1,256,256]{2,1,0:T(8,128)(2,1)S(1)} %get-tuple-element.4), channel_id=1, source_target_pairs={{0,8},{4,12},{8,0},{12,4},{1,9},{5,13},{9,1},{13,5},{2,10},{6,14},... | collective-permute-start | bytes 393224 | tf_op jit(solution)/shard_map/ppermute | solution.py:18
  136.6 2.4 %collective-permute-start.2 = (bf16[1,256,256]{2,1,0:T(8,128)(2,1)S(1)}, bf16[1,256,256]{2,1,0:T(8,128)(2,1)S(1)}, u32[]{:S(2)}, u32[]{:S(2)}) collective-permute-start(bf16[1,256,256]{2,1,0:T(8,128)(2,1)S(1)} %get-tuple-element.3), channel_id=1, source_target_pairs={{0,12},{4,8},{8,4},{12,0},{1,13},{5,9},{9,5},{13,1},{2,14},{6,10},... | collective-permute-start | bytes 393224 | tf_op jit(solution)/shard_map/ppermute | solution.py:18
  139.0 2.1 %collective-permute-done = bf16[1,256,256]{2,1,0:T(8,128)(2,1)S(1)} collective-permute-done((bf16[1,256,256]{2,1,0:T(8,128)(2,1)}, bf16[1,256,256]{2,1,0:T(8,128)(2,1)S(1)}, u32[]{:S(2)}, u32[]{:S(2)}) %collective-permute-start) | collective-permute-done | bytes 131104 | tf_op jit(solution)/shard_map/ppermute | solution.py:18
  141.2 5.9 %collective-permute-done.1 = bf16[1,256,256]{2,1,0:T(8,128)(2,1)S(1)} collective-permute-done((bf16[1,256,256]{2,1,0:T(8,128)(2,1)S(1)}, bf16[1,256,256]{2,1,0:T(8,128)(2,1)S(1)}, u32[]{:S(2)}, u32[]{:S(2)}) %collective-permute-start.1) | collective-permute-done | bytes 131104 | tf_op jit(solution)/shard_map/ppermute | solution.py:18
  147.2 2.0 %gather_fusion.1 = bf16[512,256]{1,0:T(8,128)(2,1)S(1)} fusion(bf16[1024,256]{1,0:T(8,128)(2,1)S(1)} %bitcast.74, s32[1024]{0:T(1024)S(1)} %pad_clamp_fusion), kind=kCustom, calls=%fused_computation.2 | custom fusion | bytes 526336 | tf_op jit(solution)/shard_map/gather | solution.py:84
  149.1 0.8 reshape.182
  149.9 1.0 copy.37
  150.9 1.0 copy.38
  (45 shorter events, 2.6 us)
Async XLA Ops:
  7.2 98.5 %all-gather.3.cloned.1.call-start = ((), (), s32[]{:S(2)}) async-start(), calls=%async_computation.5 | async-start | bytes 5242880 | tf_op jit(solution)/shard_map/all_gather | solution.py:72
  12.2 37.1 %copy-start = (bf16[256,2048]{1,0:T(8,128)(2,1)S(1)}, bf16[256,2048]{1,0:T(8,128)(2,1)}, u32[]{:S(2)}) copy-start(bf16[256,2048]{1,0:T(8,128)(2,1)} %param.6) | copy-start | bytes 3145732
  49.2 11.4 %copy-start.1 = (f32[256,2]{0,1:T(2,128)S(1)}, f32[256,2]{0,1:T(2,128)}, u32[]{:S(2)}) copy-start(f32[256,2]{0,1:T(2,128)} %param.11) | copy-start | bytes 6148
  49.2 20.5 %copy-start.2 = (f32[512]{0:T(512)S(1)}, f32[512]{0:T(512)}, u32[]{:S(2)}) copy-start(f32[512]{0:T(512)} %param.7) | copy-start | bytes 6148
  57.3 8.7 %all-to-all-start.4 = ((bf16[4,2,128]{2,1,0:T(2,128)(2,1)}), bf16[4,2,128]{2,1,0:T(2,128)(2,1)S(1)}, u32[]{:S(2)}, u32[]{:S(2)}) async-start(bf16[4,2,128]{2,1,0:T(2,128)(2,1)} %reshape.248), calls=%async_computation.4 | async-start | bytes 4096 | tf_op jit(solution)/shard_map/all_to_all | solution.py:63
  66.0 9.2 %all-to-all-start.2 = ((bf16[4,2,128]{2,1,0:T(2,128)(2,1)}), bf16[4,2,128]{2,1,0:T(2,128)(2,1)S(1)}, u32[]{:S(2)}, u32[]{:S(2)}) async-start(bf16[4,2,128]{2,1,0:T(2,128)(2,1)} %reshape.250), calls=%async_computation.2 | async-start | bytes 4096 | tf_op jit(solution)/shard_map/all_to_all | solution.py:66
  101.9 28.2 %all-to-all-start.1 = ((bf16[4,512,256]{2,1,0:T(8,128)(2,1)}), bf16[4,512,256]{2,1,0:T(8,128)(2,1)S(1)}, u32[]{:S(2)}, u32[]{:S(2)}) async-start(bf16[4,512,256]{2,1,0:T(8,128)(2,1)} %get-tuple-element.6), calls=%async_computation.1 | async-start | bytes 2097152 | tf_op jit(solution)/shard_map/all_to_all | solution.py:30
  134.6 6.6 %collective-permute-start = (bf16[1,256,256]{2,1,0:T(8,128)(2,1)}, bf16[1,256,256]{2,1,0:T(8,128)(2,1)S(1)}, u32[]{:S(2)}, u32[]{:S(2)}) collective-permute-start(bf16[1,256,256]{2,1,0:T(8,128)(2,1)} %get-tuple-element.5), channel_id=1, source_target_pairs={{0,4},{4,0},{8,12},{12,8},{1,5},{5,1},{9,13},{13,9},{2,6},{6,2},{1... | collective-permute-start | bytes 393224 | tf_op jit(solution)/shard_map/ppermute | solution.py:18
  134.6 12.5 %collective-permute-start.1 = (bf16[1,256,256]{2,1,0:T(8,128)(2,1)S(1)}, bf16[1,256,256]{2,1,0:T(8,128)(2,1)S(1)}, u32[]{:S(2)}, u32[]{:S(2)}) collective-permute-start(bf16[1,256,256]{2,1,0:T(8,128)(2,1)S(1)} %get-tuple-element.4), channel_id=1, source_target_pairs={{0,8},{4,12},{8,0},{12,4},{1,9},{5,13},{9,1},{13,5},{2,10},{6,14},... | collective-permute-start | bytes 393224 | tf_op jit(solution)/shard_map/ppermute | solution.py:18
  136.6 10.5 %collective-permute-start.2 = (bf16[1,256,256]{2,1,0:T(8,128)(2,1)S(1)}, bf16[1,256,256]{2,1,0:T(8,128)(2,1)S(1)}, u32[]{:S(2)}, u32[]{:S(2)}) collective-permute-start(bf16[1,256,256]{2,1,0:T(8,128)(2,1)S(1)} %get-tuple-element.3), channel_id=1, source_target_pairs={{0,12},{4,8},{8,4},{12,0},{1,13},{5,9},{9,5},{13,1},{2,14},{6,10},... | collective-permute-start | bytes 393224 | tf_op jit(solution)/shard_map/ppermute | solution.py:18
Sparse Core Ops, SparseCore 0:
  49.4 33.5 all-gather.2
